TPU v7x, 32 devices: a whole 2x2x4 slice. The times are simulated.
32 devices in a mesh: grp: 2 (over x), sp: 8 (over z, y), tp: 2 (over core).
Axes of the slice: x: 2, y: 2, z: 4, core: 2. Of those that a mesh axis runs over, the one named last changes fastest.
Arguments:
- tokens: bfloat16 [8192, 2048], P(('grp', 'sp', 'tp')), parts along dimension 0, may hold values from -8 to 8
- in_gain: float32 [2048], replicated, may hold values from 0.1 to 1.9
- w_query: bfloat16 [2048, 1024], P(None, 'tp'), may hold values from -0.125 to 0.125
- w_forget: bfloat16 [2048, 1024], P(None, 'tp'), may hold values from -0.125 to 0.125
- w_value: bfloat16 [2048, 1024], P(None, 'tp'), may hold values from -1 to 1
- w_outgate: bfloat16 [2048, 1024], P(None, 'tp'), may hold values from -0.125 to 0.125
- floor_gap: float32 [1024], P('tp'), may hold values from 0 to 0.1, as said below
- extra_decay: float32 [8192, 8], P(('grp', 'sp'), 'tp'), parts along dimension 0, may hold values from -3 to 0
- out_gain: bfloat16 [1024], P('tp'), may hold values from 0.099609375 to 1.8984375
- w_output: bfloat16 [1024, 2048], P('tp'), may hold values from -0.1875 to 0.1875
Outputs:
- mixed_out: bfloat16 [8192, 2048], P(('grp', 'sp', 'tp')), parts along dimension 0
There are 2 independent parts, one for each index of `grp`. A program takes and returns all parts, laid end to end along the dimension named above; an argument that names none is the same for every part. Nothing has to cross between parts.
Inputs may be any that keep to these rules, and one draw needn't show every extreme that they name: `floor_gap`: every entry is positive.
All inputs are finite; a program needn't handle non-finite values.
Results may differ from a plain program's by a relative error of at most 0.015.
Values may be sent and summed in bfloat16 or wider, within the bound.
A program may use at most 128 MiB of HBM per device.

v0:
```python
import jax
import jax.numpy as jnp
from jax import lax
from jax.sharding import PartitionSpec as P

HEAD_K = 128
HEAD_V = 128
BLOCK = 32


epsilon = 1e-06
highest = lax.Precision.HIGHEST


def prefix(array, axis, combine, identity):
    peers, mine = (lax.axis_size(axis), lax.axis_index(axis))
    everything = jax.tree.map(
        lambda part, kind: lax.all_gather(part.astype(kind), axis),
        array,
        (jnp.bfloat16, jnp.bfloat16),
    )
    start = jax.tree.map(
        lambda part, zero: jnp.broadcast_to(jnp.asarray(zero, part.dtype), part.shape),
        array,
        identity,
    )

    def hop(k, before):
        reached = k < mine
        new = combine(
            before, jax.tree.map(lambda part, own: part[k].astype(own.dtype), everything, array)
        )
        return jax.tree.map(lambda a, b: jnp.where(reached, a, b), new, before)

    return lax.fori_loop(0, peers, hop, start)


def gate_terms(query_proj, forget_pre, value_proj, floor_gap, extra_decay):
    tok_rows = query_proj.shape[0]
    head_count = floor_gap.shape[0] // HEAD_K
    reading = jax.nn.silu(query_proj.astype(jnp.float32)).reshape(
        tok_rows, head_count, HEAD_K
    ) * HEAD_K ** (-0.5)
    pre_gate = forget_pre.astype(jnp.float32).reshape(tok_rows, head_count, HEAD_K)
    floor_part = floor_gap.reshape(head_count, HEAD_K)
    key_terms = floor_part * jax.nn.sigmoid(-pre_gate)
    log_forget = jnp.logaddexp(
        jnp.log1p(-floor_part), jnp.log(floor_part) + jax.nn.log_sigmoid(pre_gate)
    )
    log_forget = log_forget + extra_decay[:, :, None]
    values = value_proj.astype(jnp.float32).reshape(tok_rows, head_count, HEAD_V)
    return (reading, key_terms, values, log_forget)


def blockwise(reading, key_terms, values, log_forget):
    positions, head_count, key_width = reading.shape
    value_width = values.shape[-1]
    block_count = positions // BLOCK

    def to_blocks(tensor):
        return tensor.reshape(block_count, BLOCK, head_count, tensor.shape[-1]).transpose(
            0, 2, 1, 3
        )

    def from_blocks(tensor):
        return tensor.transpose(0, 2, 1, 3).reshape(positions, head_count, tensor.shape[-1])

    causal_mask = jnp.tril(jnp.ones((BLOCK, BLOCK), dtype=bool))[:, :, None]

    def advance(carried, inputs):
        carry_state, offset = carried
        read_block, key_block, value_block, gate_block = inputs
        cumulative = jnp.cumsum(gate_block, axis=1)
        across = jnp.einsum(
            "hid,hde->hie", read_block * jnp.exp(cumulative), carry_state, precision=highest
        )
        differ = cumulative[:, :, None, :] - cumulative[:, None, :, :]
        decays = jnp.exp(jnp.where(causal_mask, differ, -jnp.inf))
        scores = jnp.einsum("hid,hjd,hijd->hij", read_block, key_block, decays, precision=highest)
        within = jnp.einsum("hij,hje->hie", scores, value_block, precision=highest)
        last_sum = cumulative[:, -1:, :]
        weighted = key_block * jnp.exp(last_sum - cumulative)
        carry_state = jnp.exp(last_sum[:, 0, :, None]) * carry_state + jnp.einsum(
            "hjd,hje->hde", weighted, value_block, precision=highest
        )
        return (
            (carry_state, offset + last_sum[:, 0, :]),
            (across + within, cumulative + offset[:, None, :]),
        )

    start_state = jnp.zeros((head_count, key_width, value_width), jnp.float32)
    start_offset = jnp.zeros((head_count, key_width), jnp.float32)
    ended, produced = lax.scan(
        advance,
        (start_state, start_offset),
        (to_blocks(reading), to_blocks(key_terms), to_blocks(values), to_blocks(log_forget)),
    )
    return (from_blocks(produced[0]), from_blocks(produced[1]), ended[0], ended[1])


def combine_pair(earlier, later):
    return (earlier[0] + later[0], jnp.exp(later[0])[:, :, None] * earlier[1] + later[1])


def body(
    tokens,
    in_gain,
    w_query,
    w_forget,
    w_value,
    w_outgate,
    floor_gap,
    extra_decay,
    out_gain,
    w_output,
):
    widened = tokens.astype(jnp.float32)
    normed = (
        widened * lax.rsqrt(jnp.mean(widened * widened, axis=-1, keepdims=True) + epsilon) * in_gain
    ).astype(jnp.bfloat16)
    shard_rows = lax.all_gather(normed, "tp", axis=0, tiled=True)
    projected = jnp.stack(
        [
            jnp.dot(shard_rows, weight, preferred_element_type=jnp.float32).astype(jnp.bfloat16)
            for weight in (w_query, w_forget, w_value, w_outgate)
        ]
    )
    query_proj, forget_pre, value_proj, out_gate = (
        projected[0],
        projected[1],
        projected[2],
        projected[3],
    )
    reading, key_terms, values, log_forget = gate_terms(
        query_proj, forget_pre, value_proj, floor_gap, extra_decay
    )
    outputs, running, end_state, end_offset = blockwise(reading, key_terms, values, log_forget)
    incoming = prefix(
        (end_offset, end_state),
        "sp",
        combine_pair,
        (jnp.zeros_like(end_offset), jnp.zeros_like(end_state)),
    )
    outputs = outputs + jnp.einsum(
        "thd,hde->the", reading * jnp.exp(running), incoming[1], precision=highest
    )
    tok_rows = outputs.shape[0]
    recur_out = outputs.astype(jnp.bfloat16).reshape(tok_rows, outputs.shape[1] * outputs.shape[2])
    recur_tok, gate_tok = (
        lax.all_to_all(recur_out, "tp", split_axis=0, concat_axis=1, tiled=True),
        lax.all_to_all(out_gate, "tp", split_axis=0, concat_axis=1, tiled=True),
    )
    recur_wide = recur_tok.astype(jnp.float32)
    inv_scale = lax.rsqrt(jnp.mean(recur_wide * recur_wide, axis=-1, keepdims=True) + epsilon)
    gate_act = jax.nn.silu(gate_tok.astype(jnp.float32))
    weight_rows = lax.all_gather(w_output, "tp", axis=0, tiled=True)
    gain_piece = lax.all_gather(out_gain, "tp", axis=0, tiled=True)
    normal_piece = recur_wide * inv_scale * gain_piece.astype(jnp.float32) * gate_act
    mixed_out = jnp.dot(
        normal_piece.astype(jnp.bfloat16), weight_rows, preferred_element_type=jnp.float32
    )
    return mixed_out.astype(jnp.bfloat16)


def solution(mesh):
    in_specs = (
        P(("grp", "sp", "tp"), None),
        P(),
        P(None, "tp"),
        P(None, "tp"),
        P(None, "tp"),
        P(None, "tp"),
        P("tp"),
        P(("grp", "sp"), "tp"),
        P("tp"),
        P("tp", None),
    )
    out_specs = P(("grp", "sp", "tp"), None)
    return jax.shard_map(body, mesh=mesh, in_specs=in_specs, out_specs=out_specs, check_vma=False)
```

profile of v0, /device:TPU:0, one launch (start us, length us, event | category | flops | bytes accessed | tf_op | source)
XLA Modules:
  0.0 273.2 jit_solution(765992881078959082)
XLA Ops:
  8.2 2.5 fusion.27
  11.0 13.2 %all-gather.8.cloned.1.call-done = bf16[512,2048]{1,0:T(8,128)(2,1)} async-done(((bf16[256,2048]{1,0:T(8,128)(2,1)}), bf16[512,2048]{1,0:T(8,128)(2,1)}) %all-gather.8.cloned.1.call-update) | async-done | bytes 2097168 | tf_op jit(solution)/shard_map/all_gather | solution.py:121
  24.2 4.2 %fusion.32 = (f32[512,512]{1,0:T(8,128)}, f32[512,512]{1,0:T(8,128)}) fusion(bf16[512,2048]{1,0:T(8,128)(2,1)} %all-gather.8.cloned.1.call-done, bf16[2048,512]{1,0:T(8,128)(2,1)S(1)} %copy-done), kind=kOutput, calls=%fused_computation.59 | convolution fusion | flops 1075052544 | bytes 6291456 | tf_op jit(solution)/shard_map/dot_general | solution.py:124
  30.0 2.5 neg.42
  32.5 4.6 %fusion.36 = f32[512,512]{1,0:T(8,128)} fusion(bf16[512,2048]{1,0:T(8,128)(2,1)} %all-gather.8.cloned.1.call-done, bf16[2048,512]{1,0:T(8,128)(2,1)} %param.16), kind=kOutput, calls=%fused_computation.63 | convolution fusion | flops 1075576832 | bytes 5242880 | tf_op jit(solution)/shard_map/dot_general | solution.py:124
  37.2 2.6 mul.125
  39.7 4.5 %fusion.29 = f32[512,512]{1,0:T(8,128)} fusion(bf16[512,2048]{1,0:T(8,128)(2,1)} %all-gather.8.cloned.1.call-done, bf16[2048,512]{1,0:T(8,128)(2,1)} %param.18), kind=kOutput, calls=%fused_computation.55 | convolution fusion | flops 1074266112 | bytes 5242880 | tf_op jit(solution)/shard_map/dot_general | solution.py:124
  44.2 2.5 reshape.116
  46.7 3.2 %copy_bitcast_fusion = (f32[16,4,32,128]{3,2,1,0:T(8,128)}, f32[16,4,32,128]{3,2,1,0:T(8,128)}) fusion(f32[16,32,4,128]{3,2,1,0:T(4,128)} %mul.125, f32[16,32,4,128]{3,2,1,0:T(4,128)} %reshape.116), kind=kLoop, calls=%fused_computation.77 | loop fusion | bytes 4194304 | tf_op jit(solution)/shard_map/transpose | solution.py:61
  50.0 2.7 fusion.46
  52.6 142.5 %while.31 = (s32[]{:T(128)}, f32[4,128,128]{2,1,0:T(8,128)S(1)}, f32[4,128]{1,0:T(4,128)S(1)}, f32[16,4,32,128]{3,2,0,1:T(8,128)}, f32[16,4,32,128]{3,2,0,1:T(8,...) while((s32[]{:T(128)}, f32[4,128,128]{2,1,0:T(8,128)S(1)}, ...), condition=%wide.region_3.4_spmd.clone, body=%wide.region_1.3_spmd.clone.sunk | while | flops 60094464 | bytes 6480540 | solution.py:93
  59.1 1.8 fusion.79
  68.0 1.8 fusion.79
  76.9 1.8 fusion.79
  85.8 1.8 fusion.79
  94.7 1.8 fusion.79
  121.4 1.8 fusion.79
  130.4 1.8 fusion.79
  166.0 1.8 fusion.79
  174.9 1.8 fusion.79
  192.7 1.8 fusion.79
  196.6 1.8 all-gather.3
  198.4 4.4 %convolution_convert_fusion.1 = bf16[512,512]{1,0:T(8,128)(2,1)} fusion(bf16[512,2048]{1,0:T(8,128)(2,1)} %all-gather.8.cloned.1.call-done, bf16[2048,512]{1,0:T(8,128)(2,1)} %param.19), kind=kOutput, calls=%fused_computation.52 | convolution fusion | flops 1074003968 | bytes 4718592 | tf_op jit(solution)/shard_map/dot_general | solution.py:124
  202.8 2.0 copy.80
  206.1 2.5 exp.67
  208.7 21.1 %all-gather.2 = bf16[8,4,128]{2,1,0:T(4,128)(2,1)S(1)} all-gather(bf16[1,4,128]{2,1,0:T(4,128)(2,1)S(1)} %convert_bitcast_fusion), channel_id=2, replica_groups=mesh['grp'=2,'sp'=8,'tp'=2] {'sp'}, dimensions={0}, use_global_device_ids=true | all-gather | bytes 9216 | tf_op jit(solution)/shard_map/all_gather | solution.py:18
  229.8 7.6 %all-gather.12.cloned.1.call-done = bf16[32,128,128]{2,1,0:T(8,128)(2,1)} async-done(((bf16[4,128,128]{2,1,0:T(8,128)(2,1)}), bf16[32,128,128]{2,1,0:T(8,128)(2,1)}) %all-gather.12.cloned.1.call-update) | async-done | bytes 1048592 | tf_op jit(solution)/shard_map/all_gather | solution.py:18
  237.4 9.3 %while.32 = (s32[]{:T(128)}, f32[4,128,128]{2,1,0:T(8,128)S(1)}, s32[]{:T(128)}, bf16[8,4,128]{2,1,0:T(4,128)(2,1)S(1)}, bf16[8,4,128,128]{3,2,1,0:T(8,128)(2,1)}, /*index=5*/s32[]{:T(128)}, s32[]{:T(128)}) while((s32[]{:T(128)}, f32[4,128,128]{2,1,0:T(8,128)S(1)}, s32[]{:T(128)}, bf16[8,4,128]{2,1,0:T(4,128)(2,1)S(1)}, ...), condition=%wide.region_5.6_spmd.clone, body=%wide.region_4.5_spmd.clone.sunk | while | flops 328196 | bytes 660593 | solution.py:35
  246.7 3.6 %fusion.30 = bf16[512,4,128]{0,2,1:T(8,128)(2,1)} fusion(f32[512,4,128]{0,2,1:T(8,128)} %copy.78, f32[4,128,128]{2,1,0:T(8,128)S(1)} %get-tuple-element.157, f32[512,4,128]{2,0,1:T(8,128)} %bitcast.151, f32[512,512]{1,0:T(8,128)S(1)} %copy-done.2), kind=kOutput, calls=%fused_computation.57 | convolution fusion | flops 403439616 | bytes 3932160 | tf_op jit(solution)/shard_map/thd,hde->the/dot_general | solution.py:144
  251.5 4.2 %all_to_all.26 = bf16[2,256,512]{1,2,0:T(8,128)(2,1)S(1)} all-to-all(bf16[2,256,512]{1,2,0:T(8,128)(2,1)S(1)} %copy.79), channel_id=1, replica_groups=mesh['grp'=2,'sp'=8,'tp'=2] {'tp'}, dimensions={0} | all-to-all | bytes 1048576 | tf_op jit(solution)/shard_map/all_to_all | solution.py:150
  255.7 3.5 %all-to-all-start.1 = ((bf16[2,256,512]{1,2,0:T(8,128)(2,1)}), bf16[2,256,512]{1,2,0:T(8,128)(2,1)S(1)}, u32[]{:S(2)}, u32[]{:S(2)}) async-start(bf16[2,256,512]{1,2,0:T(8,128)(2,1)} %copy.80), calls=%async_computation.1 | async-start | bytes 1048576 | tf_op jit(solution)/shard_map/all_to_all | solution.py:151
  262.1 4.6 %convolution_convert_fusion = bf16[256,2048]{1,0:T(8,128)(2,1)} fusion(bf16[256,1024]{0,1:T(8,128)(2,1)} %fusion.42, bf16[1024,2048]{1,0:T(8,128)(2,1)} %all-gather.10.cloned.1.call-done), kind=kOutput, calls=%fused_computation.42 | convolution fusion | flops 1074266112 | bytes 5767168 | tf_op jit(solution)/shard_map/dot_general | solution.py:159
  (241 shorter events, 143.2 us)
Async XLA Ops:
  6.5 17.7 %copy-start = (bf16[2048,512]{1,0:T(8,128)(2,1)S(1)}, bf16[2048,512]{1,0:T(8,128)(2,1)}, u32[]{:S(2)}) copy-start(bf16[2048,512]{1,0:T(8,128)(2,1)} %param.17) | copy-start | bytes 6291460
  6.5 4.3 %copy-start.5 = (f32[512,4]{0,1:T(4,128)S(1)}, f32[512,4]{0,1:T(4,128)}, u32[]{:S(2)}) copy-start(f32[512,4]{0,1:T(4,128)} %param.21) | copy-start | bytes 24580
  6.5 4.4 %copy-start.4 = (f32[512]{0:T(512)S(1)}, f32[512]{0:T(512)}, u32[]{:S(2)}) copy-start(f32[512]{0:T(512)} %param.20) | copy-start | bytes 6148
  6.5 17.7 %all-gather.8.cloned.1.call-start = ((), (), s32[]{:S(2)}) async-start(), calls=%async_computation.2 | async-start | bytes 3145728 | tf_op jit(solution)/shard_map/all_gather | solution.py:121
  10.7 226.7 %all-gather.12.cloned.1.call-start = ((), (), s32[]{:S(2)}) async-start(), calls=%async_computation.4 | async-start | bytes 1179648 | tf_op jit(solution)/shard_map/all_gather | solution.py:18
  46.7 3.2 %copy-start.1 = (f32[16,32,4,128]{3,2,1,0:T(4,128)S(1)}, f32[16,32,4,128]{3,2,1,0:T(4,128)}, u32[]{:S(2)}) copy-start(f32[16,32,4,128]{3,2,1,0:T(4,128)} %neg.42) | copy-start | bytes 3145732
  195.1 1.5 copy-start.6
  195.8 66.3 %all-gather.10.cloned.1.call-start = ((), (), s32[]{:S(2)}) async-start(), calls=%async_computation.3 | async-start | bytes 6291456 | tf_op jit(solution)/shard_map/all_gather | solution.py:156
  198.4 6.4 %copy-start.3 = (f32[16,4,32,128]{3,2,0,1:T(8,128)S(1)}, f32[16,4,32,128]{3,2,0,1:T(8,128)}, u32[]{:S(2)}) copy-start(f32[16,4,32,128]{3,2,0,1:T(8,128)} %get-tuple-element.154) | copy-start | bytes 3145732
  206.1 40.6 %copy-start.2 = (f32[512,512]{1,0:T(8,128)S(1)}, f32[512,512]{1,0:T(8,128)}, u32[]{:S(2)}) copy-start(f32[512,512]{1,0:T(8,128)} %fusion.36) | copy-start | bytes 3145732
  255.7 5.2 %all-to-all-start.1 = ((bf16[2,256,512]{1,2,0:T(8,128)(2,1)}), bf16[2,256,512]{1,2,0:T(8,128)(2,1)S(1)}, u32[]{:S(2)}, u32[]{:S(2)}) async-start(bf16[2,256,512]{1,2,0:T(8,128)(2,1)} %copy.80), calls=%async_computation.1 | async-start | bytes 1048576 | tf_op jit(solution)/shard_map/all_to_all | solution.py:151
Sparse Core Ops, SparseCore 0:
  10.9 13.2 all-gather.7
  195.9 41.4 all-gather.11
  239.0 12.3 all-gather.9
where the time goes:
time: 278 us; the launch traced here: 273 us
  matrix products  97.6 us (35%)
  other arithmetic  60.1 us (22%)
  local copies, waits for them, and re-layouts  47.5 us (17%)
  blocking collectives  27.1 us (10%)
  waiting for transfers between devices  23.1 us (8%)
  between operations  13.3 us (5%)
  starting transfers between devices  3.57 us (1%)
    dot_general x16, matrix products, advance(): within = jnp.einsum('hij,hje->hie', scores, value_block, precision=highest)  28.5 us
    squeeze x32, local copies, waits for them, and re-layouts, blockwise(): lax.scan(advance, (start_state, start_offset), (to_blocks(reading), to_bl...  27.7 us
    dot_general x16, matrix products, advance(): jnp.einsum('hjd,hje->hde', weighted, value_block, precision=highest)  24.4 us
    dot_general x16, other arithmetic, advance(): jnp.einsum('hid,hjd,hijd->hij', read_block, key_block, decays, precision=...  24.2 us
    all_gather x1, blocking collectives, prefix(): lax.all_gather(part.astype(kind), axis)  21.1 us
    dot_general x16, matrix products, advance(): jnp.einsum('hid,hde->hie', read_block * jnp.exp(cumulative), carry_state,...  18.8 us
    dot_general x4, matrix products, body(): jnp.dot(shard_rows, weight, preferred_element_type=jnp.float32)  17.7 us
    all_gather x1, waiting for transfers between devices, body(): shard_rows = lax.all_gather(normed, 'tp', axis=0, tiled=True)  13.2 us
  transfers between devices with their start and end apart: 4, of which 3 were waited for; matrix products, arithmetic and copies ran while one was open for 9% of the time, Pallas kernels for 0%

commit v1 on v0

v1 whole, which is shorter than its diff:
```python
import functools

import jax
import jax.numpy as jnp
from jax import lax
from jax.experimental import pallas as pl
from jax.experimental.pallas import tpu as pltpu
from jax.sharding import PartitionSpec as P

HEAD = 128
CHUNK = 128
MESH = pl.DeviceIdType.MESH
epsilon = 1e-06
f32 = jnp.float32
bf16 = jnp.bfloat16


def dot(a, b):
    return jnp.dot(a, b, preferred_element_type=f32)


def dot_nt(a, b):
    return lax.dot_general(a, b, (((1,), (1,)), ((), ())), preferred_element_type=f32)


def dot_tn(a, b):
    return lax.dot_general(a, b, (((0,), (0,)), ((), ())), preferred_element_type=f32)


def split(x, parts):
    pieces = []
    for _ in range(parts):
        piece = x.astype(bf16)
        pieces.append(piece)
        x = x - piece.astype(f32)
    return pieces


def kernel(
    pairs,
    tokens, in_gain, w_query, w_forget, w_value, w_outgate, floor_gap, extra, out_gain, w_output,
    out,
    tok, normed, weights, wo, proj, cum_gate, cum_extra, key_up, read_down, local_out,
    starts, offsets, own_state, own_decay, end_bf, peer_bf, peer_decay, chain_in, chain_out, incoming,
    gate_send, gate_recv, square_send, square_recv, gate_own, partial,
    load_sem, wide_send, wide_recv, state_send, state_recv, chain_send, chain_recv, last_send, last_recv,
):
    half, width = tok.shape[1], tok.shape[2]
    rows = 2 * half
    chans = floor_gap.shape[1]
    heads = chans // HEAD
    chunks = rows // CHUNK
    me = lax.axis_index("tp")
    other = 1 - me
    place = lax.axis_index("sp")
    side = place % 2
    link = place // 2
    mate = place + 1 - 2 * side

    loads = [pltpu.make_async_copy(tokens, tok.at[0], load_sem.at[0])]
    order = (w_forget, w_value, w_query, w_outgate)
    for n, w in enumerate(order):
        loads.append(pltpu.make_async_copy(w, weights.at[n], load_sem.at[1 + n]))
    loads.append(pltpu.make_async_copy(w_output, wo.at[0], load_sem.at[5]))
    for copy in loads:
        copy.start()

    barrier = pltpu.get_barrier_semaphore()
    pl.semaphore_signal(barrier, inc=1, device_id={"tp": other}, device_id_type=MESH)
    pl.semaphore_signal(barrier, inc=1, device_id={"sp": mate}, device_id_type=MESH)

    @pl.when(link > 0)
    def _():
        pl.semaphore_signal(barrier, inc=1, device_id={"sp": place - 2}, device_id_type=MESH)

    @pl.when(link < pairs - 1)
    def _():
        pl.semaphore_signal(barrier, inc=1, device_id={"sp": place + 2}, device_id_type=MESH)

    peers = 2 + jnp.minimum(link, 1) + jnp.minimum(pairs - 1 - link, 1)
    pl.semaphore_wait(barrier, peers)

    def to_tp(src, dst, send, recv):
        return pltpu.make_async_remote_copy(
            src_ref=src, dst_ref=dst, send_sem=send, recv_sem=recv,
            device_id={"tp": other}, device_id_type=MESH,
        )

    def to_sp(src, dst, send, recv, target):
        return pltpu.make_async_remote_copy(
            src_ref=src, dst_ref=dst, send_sem=send, recv_sem=recv,
            device_id={"sp": target}, device_id_type=MESH,
        )

    tok_copy = to_tp(tokens, tok.at[1], wide_send.at[0], wide_recv.at[0])
    tok_copy.start()
    wo_copy = to_tp(w_output, wo.at[1], wide_send.at[1], wide_recv.at[1])

    def normalize(slot, base):
        step = 64

        def block(n, _):
            x = tok[slot, pl.ds(pl.multiple_of(n * step, step), step), :].astype(f32)
            inv = lax.rsqrt(jnp.mean(x * x, axis=-1, keepdims=True) + epsilon)
            normed[pl.ds(pl.multiple_of(base + n * step, step), step), :] = (
                x * inv * in_gain[...]
            ).astype(bf16)
            return 0

        lax.fori_loop(0, half // step, block, 0)

    loads[0].wait()
    normalize(0, me * half)
    tok_copy.wait_recv()
    wo_copy.start()
    normalize(1, other * half)

    def project(n):
        loads[1 + n].wait()
        step = 256

        def block(k, _):
            cols = pl.ds(pl.multiple_of(k * step, step), step)
            proj[n, :, cols] = dot(normed[...], weights[n, :, cols]).astype(bf16)
            return 0

        lax.fori_loop(0, chans // step, block, 0)

    project(0)
    project(1)

    later = lax.broadcasted_iota(jnp.int32, (CHUNK, CHUNK), 0)
    sooner = lax.broadcasted_iota(jnp.int32, (CHUNK, CHUNK), 1)
    mask = later >= sooner
    lower = jnp.where(mask, 1.0, 0.0).astype(bf16)

    own_state[...] = jnp.zeros_like(own_state)
    own_decay[...] = jnp.zeros_like(own_decay)

    def states(c, _):
        at = pl.ds(pl.multiple_of(c * CHUNK, CHUNK), CHUNK)
        key = floor_gap[...] / (1.0 + jnp.exp(proj[0, at, :].astype(f32)))
        gate = jnp.log1p(-key)
        summed = sum(dot(lower, piece) for piece in split(gate, 2))
        here = extra[at, :]
        wide = jnp.concatenate(
            [jnp.broadcast_to(here[:, h : h + 1], (CHUNK, HEAD)) for h in range(heads)], axis=1
        )
        extra_sum = sum(dot(lower, piece) for piece in split(wide, 3))
        cum_gate[at, :] = summed
        cum_extra[at, :] = extra_sum
        key_up[at, :] = (key * jnp.exp(-summed)).astype(bf16)
        both = summed + extra_sum
        last = both[CHUNK - 1 : CHUNK, :]
        kept = (key * jnp.exp(last - both)).astype(bf16)
        shrink = jnp.exp(last)
        offsets[c] = own_decay[0:1, :]
        own_decay[...] = own_decay[...] + last
        for h in range(heads):
            cols = slice(h * HEAD, (h + 1) * HEAD)
            state = own_state[h]
            starts[c, h] = state.astype(bf16)
            own_state[h] = state * shrink[:, cols] + dot_tn(proj[1, at, cols], kept[:, cols])
        return 0

    lax.fori_loop(0, chunks, states, 0)
    end_bf[...] = own_state[...].astype(bf16)

    decay_copy = to_sp(own_decay, peer_decay, state_send.at[heads], state_recv.at[heads], mate)
    decay_copy.start()
    state_copies = []
    for h in range(heads):
        copy = to_sp(end_bf.at[h], peer_bf.at[h], state_send.at[h], state_recv.at[h], mate)
        copy.start()
        state_copies.append(copy)

    project(2)
    project(3)

    def outputs(c, _):
        at = pl.ds(pl.multiple_of(c * CHUNK, CHUNK), CHUNK)
        query = proj[2, at, :].astype(f32)
        reading = query / (1.0 + jnp.exp(-query)) * HEAD ** (-0.5)
        extra_sum = cum_extra[at, :]
        near = reading * jnp.exp(cum_gate[at, :])
        far = near * jnp.exp(extra_sum)
        read_down[at, :] = (far * jnp.exp(offsets[c])).astype(bf16)
        near = near.astype(bf16)
        far = far.astype(bf16)
        for h in range(heads):
            cols = slice(h * HEAD, (h + 1) * HEAD)
            scores = dot_nt(near[:, cols], key_up[at, cols])
            column = extra_sum[:, cols]
            decay = jnp.where(mask, jnp.exp(column - column.T), 0.0)
            local_out[at, cols] = dot((scores * decay).astype(bf16), proj[1, at, cols]) + dot_nt(
                far[:, cols], starts[c, h]
            )
        return 0

    def compute_outputs():
        lax.fori_loop(0, chunks, outputs, 0)

    onward = [
        to_sp(chain_out.at[h], chain_in.at[h], chain_send.at[h], chain_recv.at[h], place + 2)
        for h in range(heads)
    ]
    second = side.astype(f32)
    first = 1.0 - second

    def relay():
        decay_copy.wait_recv()
        mine = own_decay[0:1, :]
        theirs = peer_decay[0:1, :]
        early = first * mine + second * theirs
        late = first * theirs + second * mine

        @pl.when(link == 0)
        def _():
            chain_in[...] = jnp.zeros_like(chain_in)

        for h in range(heads):
            cols = slice(h * HEAD, (h + 1) * HEAD)
            state_copies[h].wait_recv()

            @pl.when(link > 0)
            def _():
                onward[h].wait_recv()

            own = own_state[h]
            peer = peer_bf[h].astype(f32)
            begun = first * own + second * peer
            ended = first * peer + second * own
            before = chain_in[h].astype(f32)
            middle = jnp.exp(early[:, cols]) * before + begun

            @pl.when(link < pairs - 1)
            def _():
                chain_out[h] = (jnp.exp(late[:, cols]) * middle + ended).astype(bf16)
                onward[h].start()

            incoming[h] = (first * before + second * middle).astype(bf16)

    front = pairs // 2

    @pl.when(link >= front)
    def _():
        compute_outputs()

    relay()

    @pl.when(link < front)
    def _():
        compute_outputs()

    def finish(base):
        at = pl.ds(pl.multiple_of(base, half), half)
        pieces = []
        squares = jnp.zeros((half, 1), f32)
        for h in range(heads):
            cols = slice(h * HEAD, (h + 1) * HEAD)
            total = local_out[at, cols] + dot_nt(read_down[at, cols], incoming[h])
            total = total.astype(bf16).astype(f32)
            squares = squares + jnp.sum(total * total, axis=-1, keepdims=True)
            gate = proj[3, at, cols].astype(f32)
            gated = total * out_gain[:, cols].astype(f32) * (gate / (1.0 + jnp.exp(-gate)))
            pieces.append(gated.astype(bf16))
        return pieces, squares

    pieces, squares = finish(other * half)
    for h in range(heads):
        gate_send[:, h * HEAD : (h + 1) * HEAD] = pieces[h]
    square_send[...] = jnp.broadcast_to(squares, square_send.shape)
    gate_copy = to_tp(gate_send, gate_recv, last_send.at[0], last_recv.at[0])
    square_copy = to_tp(square_send, square_recv, last_send.at[1], last_recv.at[1])
    gate_copy.start()
    square_copy.start()

    pieces, squares = finish(me * half)
    for h in range(heads):
        gate_own[:, h * HEAD : (h + 1) * HEAD] = pieces[h]
    tile = 512
    loads[5].wait()

    def own_part(k, _):
        cols = pl.ds(pl.multiple_of(k * tile, tile), tile)
        partial[:, cols] = dot(gate_own[...], wo[0, :, cols])
        return 0

    lax.fori_loop(0, width // tile, own_part, 0)
    wo_copy.wait_recv()
    gate_copy.wait_recv()
    square_copy.wait_recv()
    scale = lax.rsqrt((squares + square_recv[:, 0:1]) / (2.0 * chans) + epsilon)

    def whole(k, _):
        cols = pl.ds(pl.multiple_of(k * tile, tile), tile)
        both = partial[:, cols] + dot(gate_recv[...], wo[1, :, cols])
        out[:, cols] = (both * scale).astype(bf16)
        return 0

    lax.fori_loop(0, width // tile, whole, 0)

    tok_copy.wait_send()
    wo_copy.wait_send()
    decay_copy.wait_send()
    for copy in state_copies:
        copy.wait_send()

    @pl.when(link < pairs - 1)
    def _():
        for copy in onward:
            copy.wait_send()

    gate_copy.wait_send()
    square_copy.wait_send()


def body(
    tokens, in_gain, w_query, w_forget, w_value, w_outgate, floor_gap, extra_decay, out_gain, w_output
):
    half, width = tokens.shape
    rows = 2 * half
    chans = floor_gap.shape[0]
    heads = chans // HEAD
    chunks = rows // CHUNK
    vmem, sem = pltpu.VMEM, pltpu.SemaphoreType.DMA
    inner = pl.BlockSpec(memory_space=pltpu.VMEM)
    outer = pl.BlockSpec(memory_space=pl.ANY)
    square = (heads, HEAD, HEAD)
    return pl.pallas_call(
        functools.partial(kernel, lax.axis_size("sp") // 2),
        out_shape=jax.ShapeDtypeStruct((half, width), bf16),
        in_specs=[outer, inner, outer, outer, outer, outer, inner, inner, inner, outer],
        out_specs=inner,
        scratch_shapes=[
            vmem((2, half, width), bf16),
            vmem((rows, width), bf16),
            vmem((4, width, chans), bf16),
            vmem((2, chans, width), bf16),
            vmem((4, rows, chans), bf16),
            vmem((rows, chans), f32),
            vmem((rows, chans), f32),
            vmem((rows, chans), bf16),
            vmem((rows, chans), bf16),
            vmem((rows, chans), f32),
            vmem((chunks,) + square, bf16),
            vmem((chunks, 1, chans), f32),
            vmem(square, f32),
            vmem((8, chans), f32),
            vmem(square, bf16),
            vmem(square, bf16),
            vmem((8, chans), f32),
            vmem(square, bf16),
            vmem(square, bf16),
            vmem(square, bf16),
            vmem((half, chans), bf16),
            vmem((half, chans), bf16),
            vmem((half, HEAD), f32),
            vmem((half, HEAD), f32),
            vmem((half, chans), bf16),
            vmem((half, width), f32),
            sem((6,)),
            sem((2,)),
            sem((2,)),
            sem((heads + 1,)),
            sem((heads + 1,)),
            sem((heads,)),
            sem((heads,)),
            sem((2,)),
            sem((2,)),
        ],
        compiler_params=pltpu.CompilerParams(
            collective_id=0, has_side_effects=True, vmem_limit_bytes=56 * 1024 * 1024
        ),
    )(
        tokens, in_gain[None, :], w_query, w_forget, w_value, w_outgate,
        floor_gap[None, :], extra_decay, out_gain[None, :], w_output,
    )


def solution(mesh):
    in_specs = (
        P(("grp", "sp", "tp"), None),
        P(),
        P(None, "tp"),
        P(None, "tp"),
        P(None, "tp"),
        P(None, "tp"),
        P("tp"),
        P(("grp", "sp"), "tp"),
        P("tp"),
        P("tp", None),
    )
    out_specs = P(("grp", "sp", "tp"), None)
    return jax.shard_map(body, mesh=mesh, in_specs=in_specs, out_specs=out_specs, check_vma=False)
```

time: 278 us -> 34.4 us (0.12)
  the two profiles are of different devices: /device:TPU:0 before, /device:TPU:27 now
where the time goes in v1:
time: 34.4 us; the launch traced here: 34.2 us
  Pallas kernels  29 us (84%)
  local copies, waits for them, and re-layouts  5.12 us (15%)
    pallas_call x1, Pallas kernels, body(): pl.pallas_call(functools.partial(kernel, lax.axis_size('sp') // 2), out_s...  29 us
    unnamed x2, local copies, waits for them, and re-layouts  3.85 us
    broadcast_in_dim x1, local copies, waits for them, and re-layouts, body(): out_gain[None, :]  1.27 us

profile of v1, /device:TPU:27, one launch (start us, length us, event | category | flops | bytes accessed | tf_op | source)
XLA Modules:
  0.0 34.2 jit_solution(17053707062299283669)
XLA Ops:
  0.0 1.3 %broadcast_in_dim.11.out_gain = bf16[1,512]{1,0:T(2,128)(2,1)} reshape(bf16[512]{0:T(512)(128)(2,1)} %param.18) | data formatting | bytes 2048 | tf_op jit(solution)/shard_map/broadcast_in_dim | solution.py:377
  1.3 1.5 %copy.11.extra = f32[512,4]{1,0:T(8,128)} copy(f32[512,4]{0,1:T(4,128)} %param.17) | data formatting | bytes 16384 | tf_op args[7]
  2.8 29.0 %shard_map.100 = bf16[256,2048]{1,0:T(8,128)(2,1)} custom-call(bf16[256,2048]{1,0:T(8,128)(2,1)} %tokens.1, f32[1,2048]{1,0:T(1,128)} %bitcast.2, bf16[2048,512]{1,0:T(8,128)(2,1)} %w_query.1, bf16[2048,512]{1,0:T(8,128)(2,1)} %w_forget.1, bf16[2048,512]{1,0:T(8,128)(2,1)} %w_value.1, bf16[2048,512]{1,0:T(8,128)(2,1)} %w_outgate.1, f32[1,512]{1,0:T(1,128)} %bitcast.3, ...), custom_call_target="tpu_custom_call" | custom-call | tf_op jit(solution)/shard_map/pallas_call | solution.py:330
  31.8 2.3 %copy.13 = bf16[256,2048]{1,0:T(8,128)(2,1)} copy(bf16[256,2048]{1,0:T(8,128)(2,1)} %shard_map.100) | data formatting | bytes 2097152

commit v2 on v1

--- a/solution.py
+++ b/solution.py
@@ -9,6 +9,7 @@
 
 HEAD = 128
 CHUNK = 128
+PIECES = 2
 MESH = pl.DeviceIdType.MESH
 epsilon = 1e-06
 f32 = jnp.float32
@@ -38,9 +39,9 @@
 
 def kernel(
     pairs,
-    tokens, in_gain, w_query, w_forget, w_value, w_outgate, floor_gap, extra, out_gain, w_output,
+    tokens, in_gain_hbm, w_query, w_forget, w_value, w_outgate, floor_hbm, extra_hbm, out_gain_hbm, w_output,
     out,
-    tok, normed, weights, wo, proj, cum_gate, cum_extra, key_up, read_down, local_out,
+    in_gain, floor_gap, extra, out_gain, tok, normed, weights, wo, proj, cum_gate, cum_extra, extra_line, key_up, read_down, local_out,
     starts, offsets, own_state, own_decay, end_bf, peer_bf, peer_decay, chain_in, chain_out, incoming,
     gate_send, gate_recv, square_send, square_recv, gate_own, partial,
     load_sem, wide_send, wide_recv, state_send, state_recv, chain_send, chain_recv, last_send, last_recv,
@@ -62,7 +63,13 @@
     for n, w in enumerate(order):
         loads.append(pltpu.make_async_copy(w, weights.at[n], load_sem.at[1 + n]))
     loads.append(pltpu.make_async_copy(w_output, wo.at[0], load_sem.at[5]))
-    for copy in loads:
+    small = [
+        pltpu.make_async_copy(src, dst, load_sem.at[6 + n])
+        for n, (src, dst) in enumerate(
+            ((in_gain_hbm, in_gain), (floor_hbm, floor_gap), (extra_hbm, extra), (out_gain_hbm, out_gain))
+        )
+    ]
+    for copy in small + loads:
         copy.start()
 
     barrier = pltpu.get_barrier_semaphore()
@@ -109,30 +116,37 @@
 
         lax.fori_loop(0, half // step, block, 0)
 
+    for copy in small:
+        copy.wait()
+    def project(n, at):
+        step = 256
+
+        def block(k, _):
+            cols = pl.ds(pl.multiple_of(k * step, step), step)
+            proj[n, at, cols] = dot(normed[at, :], weights[n, :, cols]).astype(bf16)
+            return 0
+
+        lax.fori_loop(0, chans // step, block, 0)
+
     loads[0].wait()
     normalize(0, me * half)
+    near_rows = pl.ds(pl.multiple_of(me * half, half), half)
+    far_rows = pl.ds(pl.multiple_of(other * half, half), half)
+    every = pl.ds(0, rows)
+    loads[1].wait()
+    project(0, near_rows)
     tok_copy.wait_recv()
     wo_copy.start()
     normalize(1, other * half)
-
-    def project(n):
-        loads[1 + n].wait()
-        step = 256
-
-        def block(k, _):
-            cols = pl.ds(pl.multiple_of(k * step, step), step)
-            proj[n, :, cols] = dot(normed[...], weights[n, :, cols]).astype(bf16)
-            return 0
-
-        lax.fori_loop(0, chans // step, block, 0)
-
-    project(0)
-    project(1)
+    project(0, far_rows)
+    loads[2].wait()
+    project(1, every)
 
     later = lax.broadcasted_iota(jnp.int32, (CHUNK, CHUNK), 0)
     sooner = lax.broadcasted_iota(jnp.int32, (CHUNK, CHUNK), 1)
     mask = later >= sooner
     lower = jnp.where(mask, 1.0, 0.0).astype(bf16)
+    upper = jnp.where(later <= sooner, 1.0, 0.0).astype(bf16)
 
     own_state[...] = jnp.zeros_like(own_state)
     own_decay[...] = jnp.zeros_like(own_decay)
@@ -142,11 +156,11 @@
         key = floor_gap[...] / (1.0 + jnp.exp(proj[0, at, :].astype(f32)))
         gate = jnp.log1p(-key)
         summed = sum(dot(lower, piece) for piece in split(gate, 2))
-        here = extra[at, :]
-        wide = jnp.concatenate(
-            [jnp.broadcast_to(here[:, h : h + 1], (CHUNK, HEAD)) for h in range(heads)], axis=1
+        line = sum(dot(piece, upper) for piece in split(extra[:, at], 3))
+        extra_line[c] = line
+        extra_sum = jnp.concatenate(
+            [jnp.broadcast_to(line[h : h + 1, :], (HEAD, CHUNK)).T for h in range(heads)], axis=1
         )
-        extra_sum = sum(dot(lower, piece) for piece in split(wide, 3))
         cum_gate[at, :] = summed
         cum_extra[at, :] = extra_sum
         key_up[at, :] = (key * jnp.exp(-summed)).astype(bf16)
@@ -166,16 +180,20 @@
     lax.fori_loop(0, chunks, states, 0)
     end_bf[...] = own_state[...].astype(bf16)
 
-    decay_copy = to_sp(own_decay, peer_decay, state_send.at[heads], state_recv.at[heads], mate)
+    spans = [(h, pl.ds(p * (HEAD // PIECES), HEAD // PIECES)) for h in range(heads) for p in range(PIECES)]
+    count = len(spans)
+    decay_copy = to_sp(own_decay, peer_decay, state_send.at[count], state_recv.at[count], mate)
     decay_copy.start()
     state_copies = []
-    for h in range(heads):
-        copy = to_sp(end_bf.at[h], peer_bf.at[h], state_send.at[h], state_recv.at[h], mate)
+    for n, (h, span) in enumerate(spans):
+        copy = to_sp(end_bf.at[h, span], peer_bf.at[h, span], state_send.at[n], state_recv.at[n], mate)
         copy.start()
         state_copies.append(copy)
 
-    project(2)
-    project(3)
+    loads[3].wait()
+    project(2, every)
+    loads[4].wait()
+    project(3, every)
 
     def outputs(c, _):
         at = pl.ds(pl.multiple_of(c * CHUNK, CHUNK), CHUNK)
@@ -190,8 +208,8 @@
         for h in range(heads):
             cols = slice(h * HEAD, (h + 1) * HEAD)
             scores = dot_nt(near[:, cols], key_up[at, cols])
-            column = extra_sum[:, cols]
-            decay = jnp.where(mask, jnp.exp(column - column.T), 0.0)
+            differ = extra_sum[:, cols] - extra_line[c, h : h + 1, :]
+            decay = jnp.where(mask, jnp.exp(differ), 0.0)
             local_out[at, cols] = dot((scores * decay).astype(bf16), proj[1, at, cols]) + dot_nt(
                 far[:, cols], starts[c, h]
             )
@@ -201,8 +219,8 @@
         lax.fori_loop(0, chunks, outputs, 0)
 
     onward = [
-        to_sp(chain_out.at[h], chain_in.at[h], chain_send.at[h], chain_recv.at[h], place + 2)
-        for h in range(heads)
+        to_sp(chain_out.at[h, span], chain_in.at[h, span], chain_send.at[n], chain_recv.at[n], place + 2)
+        for n, (h, span) in enumerate(spans)
     ]
     second = side.astype(f32)
     first = 1.0 - second
@@ -218,27 +236,27 @@
         def _():
             chain_in[...] = jnp.zeros_like(chain_in)
 
-        for h in range(heads):
+        for n, (h, span) in enumerate(spans):
             cols = slice(h * HEAD, (h + 1) * HEAD)
-            state_copies[h].wait_recv()
+            state_copies[n].wait_recv()
 
             @pl.when(link > 0)
             def _():
-                onward[h].wait_recv()
-
-            own = own_state[h]
-            peer = peer_bf[h].astype(f32)
+                onward[n].wait_recv()
+
+            own = own_state[h, span]
+            peer = peer_bf[h, span].astype(f32)
             begun = first * own + second * peer
             ended = first * peer + second * own
-            before = chain_in[h].astype(f32)
+            before = chain_in[h, span].astype(f32)
             middle = jnp.exp(early[:, cols]) * before + begun
 
             @pl.when(link < pairs - 1)
             def _():
-                chain_out[h] = (jnp.exp(late[:, cols]) * middle + ended).astype(bf16)
-                onward[h].start()
-
-            incoming[h] = (first * before + second * middle).astype(bf16)
+                chain_out[h, span] = (jnp.exp(late[:, cols]) * middle + ended).astype(bf16)
+                onward[n].start()
+
+            incoming[h, span] = (first * before + second * middle).astype(bf16)
 
     front = pairs // 2
 
@@ -262,9 +280,11 @@
             total = total.astype(bf16).astype(f32)
             squares = squares + jnp.sum(total * total, axis=-1, keepdims=True)
             gate = proj[3, at, cols].astype(f32)
-            gated = total * out_gain[:, cols].astype(f32) * (gate / (1.0 + jnp.exp(-gate)))
+            gated = total * gains[:, cols] * (gate / (1.0 + jnp.exp(-gate)))
             pieces.append(gated.astype(bf16))
         return pieces, squares
+
+    gains = out_gain[...].astype(f32).reshape(1, chans)
 
     pieces, squares = finish(other * half)
     for h in range(heads):
@@ -325,14 +345,18 @@
     chunks = rows // CHUNK
     vmem, sem = pltpu.VMEM, pltpu.SemaphoreType.DMA
     inner = pl.BlockSpec(memory_space=pltpu.VMEM)
-    outer = pl.BlockSpec(memory_space=pl.ANY)
+    outer = pl.BlockSpec(memory_space=pltpu.HBM)
     square = (heads, HEAD, HEAD)
     return pl.pallas_call(
         functools.partial(kernel, lax.axis_size("sp") // 2),
         out_shape=jax.ShapeDtypeStruct((half, width), bf16),
-        in_specs=[outer, inner, outer, outer, outer, outer, inner, inner, inner, outer],
+        in_specs=[outer] * 10,
         out_specs=inner,
         scratch_shapes=[
+            vmem((1, width), f32),
+            vmem((1, chans), f32),
+            vmem((heads, rows), f32),
+            vmem((chans,), bf16),
             vmem((2, half, width), bf16),
             vmem((rows, width), bf16),
             vmem((4, width, chans), bf16),
@@ -340,6 +364,7 @@
             vmem((4, rows, chans), bf16),
             vmem((rows, chans), f32),
             vmem((rows, chans), f32),
+            vmem((chunks, heads, CHUNK), f32),
             vmem((rows, chans), bf16),
             vmem((rows, chans), bf16),
             vmem((rows, chans), f32),
@@ -359,13 +384,13 @@
             vmem((half, HEAD), f32),
             vmem((half, chans), bf16),
             vmem((half, width), f32),
-            sem((6,)),
+            sem((10,)),
             sem((2,)),
             sem((2,)),
-            sem((heads + 1,)),
-            sem((heads + 1,)),
-            sem((heads,)),
-            sem((heads,)),
+            sem((heads * PIECES + 1,)),
+            sem((heads * PIECES + 1,)),
+            sem((heads * PIECES,)),
+            sem((heads * PIECES,)),
             sem((2,)),
             sem((2,)),
         ],
@@ -374,7 +399,7 @@
         ),
     )(
         tokens, in_gain[None, :], w_query, w_forget, w_value, w_outgate,
-        floor_gap[None, :], extra_decay, out_gain[None, :], w_output,
+        floor_gap[None, :], extra_decay.T, out_gain, w_output,
     )
 
 

time: 34.4 us -> 29.3 us (0.85)
  local copies, waits for them, and re-layouts: 5.12 us -> 2.3 us
  Pallas kernels: 29 us -> 26.8 us
    pallas_call x1, Pallas kernels: 29 us -> 26.8 us  [body(): pl.pallas_call(functools.partial(kernel, lax.axis_size('sp') // 2), out_s...]
    unnamed x2 -> x1, local copies, waits for them, and re-layouts: 3.85 us -> 2.3 us
    broadcast_in_dim x1 -> x0, local copies, waits for them, and re-layouts: 1.27 us -> none  [body(): out_gain[None, :]]
where the time goes in v2:
time: 29.3 us; the launch traced here: 29.1 us
  Pallas kernels  26.8 us (91%)
  local copies, waits for them, and re-layouts  2.3 us (8%)
    pallas_call x1, Pallas kernels, body(): pl.pallas_call(functools.partial(kernel, lax.axis_size('sp') // 2), out_s...  26.8 us
    unnamed x1, local copies, waits for them, and re-layouts  2.3 us

profile of v2, /device:TPU:27, one launch (start us, length us, event | category | flops | bytes accessed | tf_op | source)
XLA Modules:
  0.0 29.1 jit_solution(11337657160315286236)
XLA Ops:
  0.0 26.8 %shard_map.100 = bf16[256,2048]{1,0:T(8,128)(2,1)} custom-call(bf16[256,2048]{1,0:T(8,128)(2,1)} %tokens.1, f32[1,2048]{1,0:T(1,128)} %bitcast.3, bf16[2048,512]{1,0:T(8,128)(2,1)} %w_query.1, bf16[2048,512]{1,0:T(8,128)(2,1)} %w_forget.1, bf16[2048,512]{1,0:T(8,128)(2,1)} %w_value.1, bf16[2048,512]{1,0:T(8,128)(2,1)} %w_outgate.1, f32[1,512]{1,0:T(1,128)} %bitcast.5, ...), custom_call_target="tpu_custom_call" | custom-call | tf_op jit(solution)/shard_map/pallas_call | solution.py:350
  26.8 2.3 %copy.12 = bf16[256,2048]{1,0:T(8,128)(2,1)} copy(bf16[256,2048]{1,0:T(8,128)(2,1)} %shard_map.100) | data formatting | bytes 2097152

commit v3 on v2

--- a/solution.py
+++ b/solution.py
@@ -9,7 +9,7 @@
 
 HEAD = 128
 CHUNK = 128
-PIECES = 2
+PIECES = 4
 MESH = pl.DeviceIdType.MESH
 epsilon = 1e-06
 f32 = jnp.float32
@@ -41,7 +41,7 @@
     pairs,
     tokens, in_gain_hbm, w_query, w_forget, w_value, w_outgate, floor_hbm, extra_hbm, out_gain_hbm, w_output,
     out,
-    in_gain, floor_gap, extra, out_gain, tok, normed, weights, wo, proj, cum_gate, cum_extra, extra_line, key_up, read_down, local_out,
+    in_gain, floor_gap, extra, out_gain, tok, normed, weights, wo, proj, cum_gate, cum_extra, extra_line, key_up, gate_factor, read_down, local_out,
     starts, offsets, own_state, own_decay, end_bf, peer_bf, peer_decay, chain_in, chain_out, incoming,
     gate_send, gate_recv, square_send, square_recv, gate_own, partial,
     load_sem, wide_send, wide_recv, state_send, state_recv, chain_send, chain_recv, last_send, last_recv,
@@ -104,7 +104,7 @@
     wo_copy = to_tp(w_output, wo.at[1], wide_send.at[1], wide_recv.at[1])
 
     def normalize(slot, base):
-        step = 64
+        step = 128
 
         def block(n, _):
             x = tok[slot, pl.ds(pl.multiple_of(n * step, step), step), :].astype(f32)
@@ -119,7 +119,7 @@
     for copy in small:
         copy.wait()
     def project(n, at):
-        step = 256
+        step = 512
 
         def block(k, _):
             cols = pl.ds(pl.multiple_of(k * step, step), step)
@@ -215,8 +215,17 @@
             )
         return 0
 
+    gains = out_gain[...].astype(f32).reshape(1, chans)
+
+    def factor(c, _):
+        at = pl.ds(pl.multiple_of(c * CHUNK, CHUNK), CHUNK)
+        gate = proj[3, at, :].astype(f32)
+        gate_factor[at, :] = gains * (gate / (1.0 + jnp.exp(-gate)))
+        return 0
+
     def compute_outputs():
         lax.fori_loop(0, chunks, outputs, 0)
+        lax.fori_loop(0, chunks, factor, 0)
 
     onward = [
         to_sp(chain_out.at[h, span], chain_in.at[h, span], chain_send.at[n], chain_recv.at[n], place + 2)
@@ -279,12 +288,8 @@
             total = local_out[at, cols] + dot_nt(read_down[at, cols], incoming[h])
             total = total.astype(bf16).astype(f32)
             squares = squares + jnp.sum(total * total, axis=-1, keepdims=True)
-            gate = proj[3, at, cols].astype(f32)
-            gated = total * gains[:, cols] * (gate / (1.0 + jnp.exp(-gate)))
-            pieces.append(gated.astype(bf16))
+            pieces.append((total * gate_factor[at, cols]).astype(bf16))
         return pieces, squares
-
-    gains = out_gain[...].astype(f32).reshape(1, chans)
 
     pieces, squares = finish(other * half)
     for h in range(heads):
@@ -298,7 +303,7 @@
     pieces, squares = finish(me * half)
     for h in range(heads):
         gate_own[:, h * HEAD : (h + 1) * HEAD] = pieces[h]
-    tile = 512
+    tile = 1024
     loads[5].wait()
 
     def own_part(k, _):
@@ -366,6 +371,7 @@
             vmem((rows, chans), f32),
             vmem((chunks, heads, CHUNK), f32),
             vmem((rows, chans), bf16),
+            vmem((rows, chans), f32),
             vmem((rows, chans), bf16),
             vmem((rows, chans), f32),
             vmem((chunks,) + square, bf16),
@@ -395,7 +401,7 @@
             sem((2,)),
         ],
         compiler_params=pltpu.CompilerParams(
-            collective_id=0, has_side_effects=True, vmem_limit_bytes=56 * 1024 * 1024
+            collective_id=0, has_side_effects=True, vmem_limit_bytes=58720256
         ),
     )(
         tokens, in_gain[None, :], w_query, w_forget, w_value, w_outgate,

time: 29.3 us -> 28.2 us (0.962)
  Pallas kernels: 26.8 us -> 25.8 us
    pallas_call x1, Pallas kernels: 26.8 us -> 25.8 us  [body(): pl.pallas_call(functools.partial(kernel, lax.axis_size('sp') // 2), out_s...]
where the time goes in v3:
time: 28.2 us; the launch traced here: 28.1 us
  Pallas kernels  25.8 us (91%)
  local copies, waits for them, and re-layouts  2.3 us (8%)
    pallas_call x1, Pallas kernels, body(): pl.pallas_call(functools.partial(kernel, lax.axis_size('sp') // 2), out_s...  25.8 us
    unnamed x1, local copies, waits for them, and re-layouts  2.3 us

profile of v3, /device:TPU:27, one launch (start us, length us, event | category | flops | bytes accessed | tf_op | source)
XLA Modules:
  0.0 28.1 jit_solution(13817077503558032736)
XLA Ops:
  0.0 25.8 %shard_map.100 = bf16[256,2048]{1,0:T(8,128)(2,1)} custom-call(bf16[256,2048]{1,0:T(8,128)(2,1)} %tokens.1, f32[1,2048]{1,0:T(1,128)} %bitcast.3, bf16[2048,512]{1,0:T(8,128)(2,1)} %w_query.1, bf16[2048,512]{1,0:T(8,128)(2,1)} %w_forget.1, bf16[2048,512]{1,0:T(8,128)(2,1)} %w_value.1, bf16[2048,512]{1,0:T(8,128)(2,1)} %w_outgate.1, f32[1,512]{1,0:T(1,128)} %bitcast.5, ...), custom_call_target="tpu_custom_call" | custom-call | tf_op jit(solution)/shard_map/pallas_call | solution.py:355
  25.8 2.3 %copy.12 = bf16[256,2048]{1,0:T(8,128)(2,1)} copy(bf16[256,2048]{1,0:T(8,128)(2,1)} %shard_map.100) | data formatting | bytes 2097152
